TPU v7x, 128 devices: a whole 4x4x4 slice. The times are simulated.
128 devices in a mesh: ep: 16 (over z, x), tp: 8 (over y, core).
Axes of the slice: x: 4, y: 4, z: 4, core: 2. Of those that a mesh axis runs over, the one named last changes fastest.
Arguments:
- mix_tokens: bfloat16 [16384, 2048], P('ep'), may hold values from -6 to 6
- mix_gain: float32 [2048], replicated, may hold values from 0.1 to 1.9
- w_query: bfloat16 [2048, 2048], P(None, 'tp'), may hold values from -0.125 to 0.125
- w_forget_fwd: bfloat16 [2048, 2048], P(None, 'tp'), may hold values from -0.125 to 0.125
- w_forget_bwd: bfloat16 [2048, 2048], P(None, 'tp'), may hold values from -0.125 to 0.125
- w_value: bfloat16 [2048, 2048], P(None, 'tp'), may hold values from -0.125 to 0.125
- decay_floor: float32 [2048], P('tp'), may hold values from 0.975 to 1
- decay_shift: float32 [16384, 16], P('ep', 'tp'), may hold values from -1.3 to 0
- head_gain: float32 [128], replicated, may hold values from 0.1 to 1.9
- w_out: bfloat16 [2048, 2048], replicated, may hold values from -0.125 to 0.125
- moe_tokens: bfloat16 [6144, 2048], P('ep'), may hold values from -6 to 6
- moe_gain: float32 [2048], replicated, may hold values from 0.1 to 1.9
- routes: int32 [6144, 2], P('ep'), may hold values from 0 to 15, all different within a row; in each aligned block of 384 rows (0 to 383, 384 to 767, ...) at most 72 rows name the same one
- route_logits: float32 [6144, 2], P('ep'), may hold values from -6 to 6
- w_expert_gate: bfloat16 [16, 2048, 5120], P('ep', None, 'tp'), may hold values from -0.125 to 0.125
- w_expert_up: bfloat16 [16, 2048, 5120], P('ep', None, 'tp'), may hold values from -0.125 to 0.125
- w_expert_down: bfloat16 [16, 5120, 2048], P('ep', 'tp'), may hold values from -0.078125 to 0.078125
Outputs:
- mixed_out: bfloat16 [16384, 2048], P(('ep', 'tp'))
- moe_out: bfloat16 [6144, 2048], P('ep', 'tp')
Inputs may be any that keep to these rules, and one draw needn't show every extreme that they name: `routes`: in each aligned block of 384 rows (the rows of one index of ep) no expert is named by more than 72 rows, and in some block an expert is named by exactly 72; the two entries of a row differ.
All inputs are finite; a program needn't handle non-finite values.
Results may differ from a plain program's by a relative error of at most 0.014.
Values may be sent and summed in bfloat16 or wider, within the bound.
A program may use at most 128 MiB of HBM per device.

v0:
```python
import math

import jax
import jax.numpy as jnp
from jax import lax
from jax.sharding import Mesh
from jax.sharding import PartitionSpec as P

DK = 128
DV = 128
EP = ("ep_0", "ep_1")
EP_TP = ("ep_0", "ep_1", "tp")


EPSILON = 1e-06


def nothing_yet(value, identity):
    return jax.tree.map(
        lambda a, e: jnp.broadcast_to(jnp.asarray(e, a.dtype), a.shape), value, identity
    )


def prefix_by_axis(value, axes, combine, identity, reverse):
    before = start = nothing_yet(value, identity)
    total = value
    for axis in reversed(axes):
        count, index = (lax.axis_size(axis), lax.axis_index(axis))
        pieces = jax.tree.map(
            lambda part, kind: lax.all_gather(part.astype(kind), axis),
            total,
            (jnp.bfloat16, jnp.bfloat16),
        )
        inside, total = (start, start)
        for k in reversed(range(count)) if reverse else range(count):
            passed = k > index if reverse else k < index
            total = combine(
                total, jax.tree.map(lambda part, own: part[k].astype(own.dtype), pieces, value)
            )
            inside = jax.tree.map(lambda new, old: jnp.where(passed, new, old), total, inside)
        before = combine(inside, before)
    return before


def rms_rows(array, norm_gain):
    floats = array.astype(jnp.float32)
    factor = lax.rsqrt(jnp.mean(floats * floats, axis=-1, keepdims=True) + EPSILON)
    return floats * factor * norm_gain


def decay_terms(pre_act, lower_bound, shifts, head_count):
    squashed = jax.nn.sigmoid(pre_act.astype(jnp.float32))
    key_rows = (1.0 - lower_bound)[None, :] * (1.0 - squashed)
    key_rows = key_rows.reshape(key_rows.shape[0], head_count, key_rows.shape[1] // head_count)
    log_decay = jnp.log1p(-key_rows) + shifts[:, :, None]
    return (key_rows, log_decay)


def sweep_forward(queries, key_rows, values, log_decay, blk_rows):
    token_count, head_count, key_width = queries.shape
    value_width = values.shape[2]
    block_count = token_count // blk_rows
    lower_mask = jnp.tril(jnp.ones((blk_rows, blk_rows), jnp.float32))

    def to_blocks(array):
        return array.reshape(block_count, blk_rows, head_count, array.shape[2])

    def advance(carried, block):
        states, offset = carried
        block_q, block_k, block_v, block_g = block
        running = jnp.cumsum(block_g, axis=0)
        query_grown = block_q * jnp.exp(running)
        key_shrunk = block_k * jnp.exp(-running)
        scores = jnp.einsum("thd,shd->hts", query_grown, key_shrunk) * lower_mask[None]
        result = jnp.einsum("hts,shv->thv", scores, block_v) + jnp.einsum(
            "thd,hdv->thv", query_grown, states
        )
        block_end = running[-1]
        states = jnp.exp(block_end)[:, :, None] * states + jnp.einsum(
            "shd,shv->hdv", block_k * jnp.exp(block_end[None] - running), block_v
        )
        return ((states, offset + block_end), (result, offset[None] + running))

    starting = (
        jnp.zeros((head_count, key_width, value_width), jnp.float32),
        jnp.zeros((head_count, key_width), jnp.float32),
    )
    blocks_in = (to_blocks(queries), to_blocks(key_rows), to_blocks(values), to_blocks(log_decay))
    (states, totals), (results, cumulative) = lax.scan(advance, starting, blocks_in)
    return (
        results.reshape(token_count, head_count, value_width),
        cumulative.reshape(token_count, head_count, key_width),
        totals,
        states,
    )


def sweep_back(queries, key_rows, values, log_decay, blk_rows):
    token_count, head_count, key_width = queries.shape
    value_width = values.shape[2]
    block_count = token_count // blk_rows
    upper_mask = jnp.triu(jnp.ones((blk_rows, blk_rows), jnp.float32))

    def to_blocks(array):
        return array.reshape(block_count, blk_rows, head_count, array.shape[2])

    def advance(carried, block):
        states, offset = carried
        block_q, block_k, block_v, block_g = block
        block_sum = jnp.sum(block_g, axis=0)
        suffix = block_sum[None] - jnp.cumsum(block_g, axis=0) + block_g
        query_grown = block_q * jnp.exp(suffix)
        key_shrunk = block_k * jnp.exp(-suffix)
        scores = jnp.einsum("thd,shd->hts", query_grown, key_shrunk) * upper_mask[None]
        result = jnp.einsum("hts,shv->thv", scores, block_v) + jnp.einsum(
            "thd,hdv->thv", query_grown, states
        )
        states = jnp.exp(block_sum)[:, :, None] * states + jnp.einsum(
            "shd,shv->hdv", block_k * jnp.exp(block_sum[None] - suffix), block_v
        )
        return ((states, offset + block_sum), (result, offset[None] + suffix))

    starting = (
        jnp.zeros((head_count, key_width, value_width), jnp.float32),
        jnp.zeros((head_count, key_width), jnp.float32),
    )
    blocks_in = (to_blocks(queries), to_blocks(key_rows), to_blocks(values), to_blocks(log_decay))
    (states, totals), (results, cumulative) = lax.scan(advance, starting, blocks_in, reverse=True)
    return (
        results.reshape(token_count, head_count, value_width),
        cumulative.reshape(token_count, head_count, key_width),
        totals,
        states,
    )


def chain_join(earlier, later):
    return (earlier[0] + later[0], jnp.exp(later[0])[:, :, None] * earlier[1] + later[1])


def slot_positions(route_rows, expert_count, capacity):
    flattened = route_rows.reshape(-1)
    onehot = (flattened[:, None] == jnp.arange(expert_count, dtype=jnp.int32)[None, :]).astype(
        jnp.int32
    )
    before = jnp.cumsum(onehot, axis=0) - onehot
    slot_rank = jnp.sum(before * onehot, axis=1)
    return (flattened * capacity + slot_rank).reshape(route_rows.shape)


def body(
    mix_tokens,
    mix_gain,
    w_query,
    w_forget_fwd,
    w_forget_bwd,
    w_value,
    decay_floor,
    decay_shift,
    head_gain,
    w_out,
    moe_tokens,
    moe_gain,
    routes,
    route_logits,
    w_expert_gate,
    w_expert_up,
    w_expert_down,
):
    tp_size = lax.axis_size("tp")
    ep_size = lax.axis_size(EP)
    seg_rows = mix_tokens.shape[0]
    head_count = w_query.shape[1] // DK
    blk_rows = math.gcd(seg_rows, 128)
    normed = rms_rows(mix_tokens, mix_gain).astype(jnp.bfloat16)

    def project(weight):
        return jnp.dot(normed, weight, preferred_element_type=jnp.float32).astype(jnp.bfloat16)

    queries = jax.nn.silu(project(w_query).astype(jnp.float32)).reshape(seg_rows, head_count, DK)
    values = project(w_value).astype(jnp.float32).reshape(seg_rows, head_count, DV)
    keys_fwd, forward_log_decay = decay_terms(
        project(w_forget_fwd), decay_floor, decay_shift, head_count
    )
    keys_bwd, logs_bwd = decay_terms(project(w_forget_bwd), decay_floor, decay_shift, head_count)
    out_fwd, cum_fwd, total_fwd, summary_fwd = sweep_forward(
        queries, keys_fwd, values, forward_log_decay, blk_rows
    )
    out_bwd, cum_bwd, total_bwd, summary_bwd = sweep_back(
        queries, keys_bwd, values, logs_bwd, blk_rows
    )
    identity = (jnp.zeros_like(total_fwd), jnp.zeros_like(summary_fwd))
    incoming_fwd = prefix_by_axis((total_fwd, summary_fwd), EP, chain_join, identity, False)[1]
    incoming_bwd = prefix_by_axis((total_bwd, summary_bwd), EP, chain_join, identity, True)[1]
    grown_both = jnp.stack([queries * jnp.exp(cum_fwd), queries * jnp.exp(cum_bwd)], axis=2)
    carried_both = jnp.stack([incoming_fwd, incoming_bwd], axis=1)
    combined = out_fwd + out_bwd + jnp.einsum("thed,hedv->thv", grown_both, carried_both)
    readout = rms_rows(combined, head_gain).reshape(seg_rows, head_count * DV).astype(jnp.bfloat16)
    regrouped = lax.all_to_all(readout, "tp", split_axis=0, concat_axis=1, tiled=True)
    mixed_out = jnp.dot(regrouped, w_out, preferred_element_type=jnp.float32).astype(jnp.bfloat16)
    token_rows = moe_tokens.shape[0]
    model_cols = moe_tokens.shape[1]
    pick_count = routes.shape[1]
    capacity = 3 * token_rows // ep_size
    part_cols = model_cols // tp_size
    normed_moe = rms_rows(moe_tokens, moe_gain).astype(jnp.bfloat16)
    position = slot_positions(routes, ep_size, capacity)
    local_rows = jnp.arange(pick_count * token_rows, dtype=jnp.int32) // pick_count
    slot_token = (
        jnp.full((ep_size * capacity,), token_rows, jnp.int32)
        .at[position.reshape(-1)]
        .set(local_rows)
    )
    gate_weight = w_expert_gate[0]
    up_weight = w_expert_up[0]
    down_weight = w_expert_down[0]
    own_cols = lax.dynamic_slice_in_dim(normed_moe, lax.axis_index("tp") * part_cols, part_cols, 1)
    padded = jnp.concatenate([own_cols, jnp.zeros((1, part_cols), jnp.bfloat16)], axis=0)
    outgoing = padded[slot_token].reshape(ep_size, capacity, part_cols)
    arrived = lax.all_to_all(outgoing, EP, split_axis=0, concat_axis=0, tiled=True)
    pieces = lax.all_gather(arrived, "tp", axis=2, tiled=True)
    flattened = pieces.reshape(-1, pieces.shape[2])
    gate_acts = jnp.dot(flattened, gate_weight, preferred_element_type=jnp.float32)
    up_acts = jnp.dot(flattened, up_weight, preferred_element_type=jnp.float32)
    hidden = (jax.nn.silu(gate_acts) * up_acts).astype(jnp.bfloat16)
    partial_value = jnp.dot(hidden, down_weight, preferred_element_type=jnp.float32)
    summed = lax.psum_scatter(
        partial_value.astype(jnp.bfloat16), "tp", scatter_dimension=1, tiled=True
    )
    returned = lax.all_to_all(
        summed.reshape(ep_size, capacity, part_cols), EP, split_axis=0, concat_axis=0, tiled=True
    )
    flat_back = returned.reshape(ep_size * capacity, part_cols)
    picked = flat_back[position].astype(jnp.float32)
    weights = jax.nn.sigmoid(route_logits - jnp.flip(route_logits, 1))
    moe_out = jnp.sum(picked * weights[:, :, None], axis=1).astype(jnp.bfloat16)
    return (mixed_out, moe_out)


def solution(mesh):
    finer = Mesh(mesh.devices.reshape(4, 4, mesh.shape["tp"]), ("ep_0", "ep_1", "tp"))
    return jax.shard_map(
        body,
        mesh=finer,
        in_specs=(
            P(EP, None),
            P(),
            P(None, "tp"),
            P(None, "tp"),
            P(None, "tp"),
            P(None, "tp"),
            P("tp"),
            P(EP, "tp"),
            P(),
            P(),
            P(EP, None),
            P(),
            P(EP, None),
            P(EP, None),
            P(EP, None, "tp"),
            P(EP, None, "tp"),
            P(EP, "tp", None),
        ),
        out_specs=(P(EP_TP, None), P(EP, "tp")),
        check_vma=False,
    )
```

profile of v0, /device:TPU:0, one launch (start us, length us, event | category | flops | bytes accessed | tf_op | source)
XLA Modules:
  0.0 330.4 jit_solution(3483865044686736720)
XLA Ops:
  7.2 3.6 %convert_element_type.559 = f32[384,2048]{1,0:T(8,128)} convert(bf16[384,2048]{1,0:T(8,128)(2,1)} %param.31) | non-fusion elementwise | flops 786432 | bytes 4718592 | tf_op jit(solution)/shard_map/convert_element_type | solution.py:46
  14.8 3.4 %scatter_custom_fusion = s32[1152]{0:T(1024)S(1)} fusion(s32[768]{0:T(1024)S(1)} %fusion.161, s32[768]{0:T(1024)S(1)} %add_select_fusion, s32[]{:T(128)} %constant.148.clone.1), kind=kCustom, calls=%fused_computation.233 | custom fusion | bytes 4612 | tf_op jit(solution)/shard_map/scatter | solution.py:212
  20.2 4.6 %gather_fusion = bf16[1152,256]{1,0:T(8,128)(2,1)} fusion(bf16[385,256]{1,0:T(8,128)(2,1)S(1)} %concatenate.3, s32[2048]{0:T(1024)S(1)} %pad_clamp_fusion), kind=kCustom, calls=%fused_computation | custom fusion | bytes 1184256 | tf_op jit(solution)/shard_map/gather | solution.py:219
  24.8 8.0 %all-to-all-start.1 = ((bf16[16,72,256]{2,1,0:T(8,128)(2,1)}), bf16[16,72,256]{2,1,0:T(8,128)(2,1)S(1)}, u32[]{:S(2)}, u32[]{:S(2)}) async-start(bf16[16,72,256]{2,1,0:T(8,128)(2,1)} %bitcast.468), calls=%async_computation.1 | async-start | bytes 1179648 | tf_op jit(solution)/shard_map/all_to_all | solution.py:220
  33.1 3.2 fusion.60
  59.7 5.4 %log-plus-one_add_fusion.1 = (f32[8,128,2,128]{3,2,1,0:T(2,128)}, f32[8,128,2,128]{3,2,1,0:T(2,128)}) fusion(f32[8,128,2,128]{3,2,1,0:T(2,128)} %reshape_reshape.17, f32[8,128,2]{2,1,0:T(8,128)} %bitcast.469, f32[8,128,2,128]{3,2,1,0:T(2,128)} %reshape_reshape.21), kind=kLoop, calls=%fused_computation.128 | loop fusion | flops 1048576 | bytes 4202496 | tf_op jit(solution)/shard_map/add | solution.py:55
  68.7 48.9 %while.38 = (s32[]{:T(128)}, f32[2,128,128]{2,1,0:T(8,128)S(1)}, f32[2,128]{1,0:T(2,128)S(1)}, f32[8,128,2,128]{1,3,2,0:T(8,128)}, f32[8,128,2,128]{3,2,1,0:T(2,...) while((s32[]{:T(128)}, f32[2,128,128]{2,1,0:T(8,128)S(1)}, ...), condition=%wide.region_3.4_spmd.clone, body=%wide.region_1.3_spmd.clone.sunk | while | flops 38273536 | bytes 2437757 | solution.py:89
  117.6 8.6 %fusion.66 = f32[1152,640]{1,0:T(8,128)} fusion(bf16[1152,2048]{1,0:T(8,128)(2,1)} %bitcast.474, bf16[1,2048,640]{2,1,0:T(8,128)(2,1)} %param.35), kind=kOutput, calls=%fused_computation.91 | convolution fusion | flops 3019898880 | bytes 10289152 | tf_op jit(solution)/shard_map/dot_general | solution.py:223
  126.2 13.2 %convolution_convert_fusion = bf16[1152,2048]{1,0:T(8,128)(2,1)} fusion(bf16[1,640,2048]{2,1,0:T(8,128)(2,1)S(1)} %copy-done, bf16[1152,2048]{1,0:T(8,128)(2,1)} %bitcast.475, f32[1152,640]{1,0:T(8,128)} %fusion.66, bf16[1,2048,640]{2,1,0:T(8,128)(2,1)} %param.36), kind=kOutput, calls=%fused_computation.85 | convolution fusion | flops 6046580736 | bytes 17629184 | tf_op jit(solution)/shard_map/dot_general | solution.py:226
  141.8 50.8 %while.39 = (s32[]{:T(128)}, f32[2,128,128]{2,1,0:T(8,128)S(1)}, f32[2,128]{1,0:T(2,128)S(1)}, f32[8,128,2,128]{1,3,2,0:T(8,128)}, f32[8,128,2,128]{3,2,1,0:T(2,...) while((s32[]{:T(128)}, f32[2,128,128]{2,1,0:T(8,128)S(1)}, ...), condition=%wide.region_7.8_spmd.clone, body=%wide.region_4.7_spmd.clone.sunk | while | flops 38437124 | bytes 3094181 | solution.py:128
  194.2 13.0 %all-gather.1 = bf16[8,128,128]{2,1,0:T(8,128)(2,1)S(1)} all-gather(bf16[2,128,128]{2,1,0:T(8,128)(2,1)S(1)} %convert_element_type.502), channel_id=3, replica_groups=mesh['ep_0'=4,'ep_1'=4,'tp'=8] {'ep_1'}, dimensions={0}, use_global_device_ids=true | all-gather | bytes 327680 | tf_op jit(solution)/shard_map/all_gather | solution.py:30
  207.8 9.6 %all-gather.4 = bf16[4,2,128]{2,1,0:T(2,128)(2,1)S(1)} all-gather(bf16[1,2,128]{2,1,0:T(2,128)(2,1)S(1)} %convert_bitcast_fusion.17), channel_id=2, replica_groups=mesh['ep_0'=4,'ep_1'=4,'tp'=8] {'ep_1'}, dimensions={0}, use_global_device_ids=true | all-gather | bytes 2560 | tf_op jit(solution)/shard_map/all_gather | solution.py:30
  217.6 12.5 %all_gather.48 = bf16[4,2,128,128]{3,2,1,0:T(8,128)(2,1)S(1)} all-gather(bf16[1,2,128,128]{3,2,1,0:T(8,128)(2,1)S(1)} %copy.121), channel_id=1, replica_groups=mesh['ep_0'=4,'ep_1'=4,'tp'=8] {'ep_0'}, dimensions={0}, use_global_device_ids=true | all-gather | bytes 327680 | tf_op jit(solution)/shard_map/all_gather | solution.py:30
  230.6 12.3 %all-gather.3 = bf16[8,128,128]{2,1,0:T(8,128)(2,1)S(1)} all-gather(bf16[2,128,128]{2,1,0:T(8,128)(2,1)S(1)} %convert_element_type.534), channel_id=5, replica_groups=mesh['ep_0'=4,'ep_1'=4,'tp'=8] {'ep_1'}, dimensions={0}, use_global_device_ids=true | all-gather | bytes 327680 | tf_op jit(solution)/shard_map/all_gather | solution.py:30
  243.4 7.0 %all-gather.5 = bf16[4,2,128]{2,1,0:T(2,128)(2,1)S(1)} all-gather(bf16[1,2,128]{2,1,0:T(2,128)(2,1)S(1)} %convert_bitcast_fusion.16), channel_id=4, replica_groups=mesh['ep_0'=4,'ep_1'=4,'tp'=8] {'ep_1'}, dimensions={0}, use_global_device_ids=true | all-gather | bytes 2560 | tf_op jit(solution)/shard_map/all_gather | solution.py:30
  250.7 12.5 %all_gather.54 = bf16[4,2,128,128]{3,2,1,0:T(8,128)(2,1)S(1)} all-gather(bf16[1,2,128,128]{3,2,1,0:T(8,128)(2,1)S(1)} %copy.134), channel_id=1, replica_groups=mesh['ep_0'=4,'ep_1'=4,'tp'=8] {'ep_0'}, dimensions={0}, use_global_device_ids=true | all-gather | bytes 327680 | tf_op jit(solution)/shard_map/all_gather | solution.py:30
  265.1 9.5 %all_gather.45 = bf16[4,2,128]{2,1,0:T(2,128)(2,1)S(1)} all-gather(bf16[1,2,128]{2,1,0:T(2,128)(2,1)S(1)} %get-tuple-element.469), channel_id=1, replica_groups=mesh['ep_0'=4,'ep_1'=4,'tp'=8] {'ep_0'}, dimensions={0}, use_global_device_ids=true | all-gather | bytes 2560 | tf_op jit(solution)/shard_map/all_gather | solution.py:30
  274.6 7.0 %all_gather.51 = bf16[4,2,128]{2,1,0:T(2,128)(2,1)S(1)} all-gather(bf16[1,2,128]{2,1,0:T(2,128)(2,1)S(1)} %get-tuple-element.479), channel_id=1, replica_groups=mesh['ep_0'=4,'ep_1'=4,'tp'=8] {'ep_0'}, dimensions={0}, use_global_device_ids=true | all-gather | bytes 2560 | tf_op jit(solution)/shard_map/all_gather | solution.py:30
  283.8 4.5 %all-to-all-start = ((bf16[8,128,256]{1,2,0:T(8,128)(2,1)}), bf16[8,128,256]{1,2,0:T(8,128)(2,1)S(1)}, u32[]{:S(2)}, u32[]{:S(2)}) async-start(bf16[8,128,256]{1,2,0:T(8,128)(2,1)} %copy.146), calls=%async_computation | async-start | bytes 1048576 | tf_op jit(solution)/shard_map/all_to_all | solution.py:199
  288.6 10.0 %all-to-all-done = bf16[8,128,256]{1,2,0:T(8,128)(2,1)S(1)} async-done(((bf16[8,128,256]{1,2,0:T(8,128)(2,1)}), bf16[8,128,256]{1,2,0:T(8,128)(2,1)S(1)}, u32[]{:S(2)}, u32[]{:S(2)}) %all-to-all-start) | async-done | bytes 524320 | tf_op jit(solution)/shard_map/all_to_all | solution.py:199
  299.5 4.9 %all-to-all-start.2 = ((bf16[16,72,256]{2,1,0:T(8,128)(2,1)}), bf16[16,72,256]{2,1,0:T(8,128)(2,1)S(1)}, u32[]{:S(2)}, u32[]{:S(2)}) async-start(bf16[16,72,256]{2,1,0:T(8,128)(2,1)} %bitcast.472), calls=%async_computation.3 | async-start | bytes 1179648 | tf_op jit(solution)/shard_map/all_to_all | solution.py:230
  305.2 5.8 %convolution_convert_fusion.1 = bf16[128,2048]{1,0:T(8,128)(2,1)} fusion(bf16[128,2048]{0,1:T(8,128)(2,1)} %bitcast.465, bf16[2048,2048]{1,0:T(8,128)(2,1)} %param.30), kind=kOutput, calls=%fused_computation.93 | convolution fusion | flops 1074003968 | bytes 9437184 | tf_op jit(solution)/shard_map/dot_general | solution.py:200
  311.0 5.3 %all-to-all-done.2 = bf16[16,72,256]{2,1,0:T(8,128)(2,1)S(1)} async-done(((bf16[16,72,256]{2,1,0:T(8,128)(2,1)}), bf16[16,72,256]{2,1,0:T(8,128)(2,1)S(1)}, u32[]{:S(2)}, u32[]{:S(2)}) %all-to-all-start.2) | async-done | bytes 589856 | tf_op jit(solution)/shard_map/all_to_all | solution.py:230
  316.3 3.3 gather_fusion.1
  (295 shorter events, 148.0 us)
Async XLA Ops:
  7.2 119.1 %copy-start = (bf16[1,640,2048]{2,1,0:T(8,128)(2,1)S(1)}, bf16[1,640,2048]{2,1,0:T(8,128)(2,1)}, u32[]{:S(2)}) copy-start(bf16[1,640,2048]{2,1,0:T(8,128)(2,1)} %param.37) | copy-start | bytes 7864324
  7.2 3.6 %copy-start.4 = (bf16[384,2048]{1,0:T(8,128)(2,1)S(1)}, bf16[384,2048]{1,0:T(8,128)(2,1)}, u32[]{:S(2)}) copy-start(bf16[384,2048]{1,0:T(8,128)(2,1)} %param.31) | copy-start | bytes 4718596
  7.2 4.0 %copy-start.17 = (s32[384,2]{0,1:T(2,128)S(1)}, s32[384,2]{0,1:T(2,128)}, u32[]{:S(2)}) copy-start(s32[384,2]{0,1:T(2,128)} %param.33) | copy-start | bytes 9220
  20.2 16.1 %copy-start.18 = (f32[256]{0:T(256)S(1)}, f32[256]{0:T(256)}, u32[]{:S(2)}) copy-start(f32[256]{0:T(256)} %param.27) | copy-start | bytes 3076
  20.2 16.2 %copy-start.15 = (f32[2048]{0:T(1024)S(1)}, f32[2048]{0:T(1024)}, u32[]{:S(2)}) copy-start(f32[2048]{0:T(1024)} %param.22) | copy-start | bytes 24580
  24.8 40.3 %all-to-all-start.1 = ((bf16[16,72,256]{2,1,0:T(8,128)(2,1)}), bf16[16,72,256]{2,1,0:T(8,128)(2,1)S(1)}, u32[]{:S(2)}, u32[]{:S(2)}) async-start(bf16[16,72,256]{2,1,0:T(8,128)(2,1)} %bitcast.468), calls=%async_computation.1 | async-start | bytes 1179648 | tf_op jit(solution)/shard_map/all_to_all | solution.py:220
  32.8 84.8 %all-gather.8.cloned.1.call-start = ((), (), s32[]{:S(2)}) async-start(), calls=%async_computation.4 | async-start | bytes 5308416 | tf_op jit(solution)/shard_map/all_gather | solution.py:221
  33.1 3.5 %copy-start.2 = (bf16[1024,2048]{1,0:T(8,128)(2,1)S(1)}, bf16[1024,2048]{1,0:T(8,128)(2,1)}, u32[]{:S(2)}) copy-start(bf16[1024,2048]{1,0:T(8,128)(2,1)} %param.21) | copy-start | bytes 12582916
  40.0 2.3 copy-start.22
  42.2 2.3 copy-start.23
  44.6 7.5 %copy-start.16 = (f32[1024,2]{0,1:T(2,128)S(1)}, f32[1024,2]{0,1:T(2,128)}, u32[]{:S(2)}) copy-start(f32[1024,2]{0,1:T(2,128)} %param.28) | copy-start | bytes 24580
  66.0 232.7 %reduce-scatter.2.cloned.1.call-start = ((), (), s32[]{:S(2)}) async-start(), calls=%async_computation.5 | async-start | bytes 5308416 | tf_op jit(solution)/shard_map/reduce_scatter | solution.py:227
  139.4 2.4 copy-start.3
  141.8 50.8 %copy-start.6 = (f32[1024,256]{1,0:T(8,128)S(1)}, f32[1024,256]{1,0:T(8,128)}, u32[]{:S(2)}) copy-start(f32[1024,256]{1,0:T(8,128)} %convert_multiply_fusion.2) | copy-start | bytes 3145732
  192.7 71.1 %copy-start.7 = (f32[8,128,2,128]{3,2,1,0:T(2,128)S(1)}, f32[8,128,2,128]{3,2,1,0:T(2,128)}, u32[]{:S(2)}) copy-start(f32[8,128,2,128]{3,2,1,0:T(2,128)} %get-tuple-element.265) | copy-start | bytes 3145732
  230.1 34.3 %copy-start.8 = (f32[8,128,2,128]{3,2,1,0:T(2,128)S(1)}, f32[8,128,2,128]{3,2,1,0:T(2,128)}, u32[]{:S(2)}) copy-start(f32[8,128,2,128]{3,2,1,0:T(2,128)} %get-tuple-element.264) | copy-start | bytes 3145732
  264.3 17.6 %copy-start.9 = (f32[1024,2,1,128]{3,1,0,2:T(2,128)S(1)}, f32[1024,2,1,128]{3,1,0,2:T(2,128)}, u32[]{:S(2)}) copy-start(f32[1024,2,1,128]{3,1,0,2:T(2,128)} %reshape.725) | copy-start | bytes 3145732
  265.0 17.1 %copy-start.10 = (f32[8,128,2,128]{1,3,2,0:T(8,128)S(1)}, f32[8,128,2,128]{1,3,2,0:T(8,128)}, u32[]{:S(2)}) copy-start(f32[8,128,2,128]{1,3,2,0:T(8,128)} %get-tuple-element.259) | copy-start | bytes 3145732
  265.0 17.1 %copy-start.11 = (f32[8,128,2,128]{1,3,2,0:T(8,128)S(1)}, f32[8,128,2,128]{1,3,2,0:T(8,128)}, u32[]{:S(2)}) copy-start(f32[8,128,2,128]{1,3,2,0:T(8,128)} %get-tuple-element.258) | copy-start | bytes 3145732
  282.1 6.2 %copy-start.13 = (s32[384,2]{1,0:T(8,128)S(1)}, s32[384,2]{1,0:T(8,128)}, u32[]{:S(2)}) copy-start(s32[384,2]{1,0:T(8,128)} %get-tuple-element.463) | copy-start | bytes 9220
  282.1 6.4 %copy-start.14 = (f32[384,2]{0,1:T(2,128)S(1)}, f32[384,2]{0,1:T(2,128)}, u32[]{:S(2)}) copy-start(f32[384,2]{0,1:T(2,128)} %param.34) | copy-start | bytes 9220
  283.8 14.8 %all-to-all-start = ((bf16[8,128,256]{1,2,0:T(8,128)(2,1)}), bf16[8,128,256]{1,2,0:T(8,128)(2,1)S(1)}, u32[]{:S(2)}, u32[]{:S(2)}) async-start(bf16[8,128,256]{1,2,0:T(8,128)(2,1)} %copy.146), calls=%async_computation | async-start | bytes 1048576 | tf_op jit(solution)/shard_map/all_to_all | solution.py:199
  299.5 16.8 %all-to-all-start.2 = ((bf16[16,72,256]{2,1,0:T(8,128)(2,1)}), bf16[16,72,256]{2,1,0:T(8,128)(2,1)S(1)}, u32[]{:S(2)}, u32[]{:S(2)}) async-start(bf16[16,72,256]{2,1,0:T(8,128)(2,1)} %bitcast.472), calls=%async_computation.3 | async-start | bytes 1179648 | tf_op jit(solution)/shard_map/all_to_all | solution.py:230
  305.2 18.4 %copy-start.1 = (bf16[1,640,2048]{2,1,0:T(8,128)(2,1)S(1)}, bf16[1,640,2048]{2,1,0:T(8,128)(2,1)}, u32[]{:S(2)}) copy-start(bf16[1,640,2048]{2,1,0:T(8,128)(2,1)} %param.37) | copy-start | bytes 7864324
  (5 other events, 5.9 us)
Sparse Core Ops, SparseCore 0:
  66.1 39.4 all-gather.7
  139.5 40.8 reduce-scatter.1
where the time goes:
time: 333 us; the launch traced here: 330 us
  matrix products  86.5 us (26%)
  blocking collectives  83.3 us (25%)
  other arithmetic  70.3 us (21%)
  local copies, waits for them, and re-layouts  41.6 us (12%)
  starting transfers between devices  17.8 us (5%)
  waiting for transfers between devices  15.4 us (5%)
  between operations  14.8 us (4%)
    all_gather x8, blocking collectives, prefix_by_axis(): lax.all_gather(part.astype(kind), axis)  83.3 us
    dot_general x16, matrix products, advance(): jnp.einsum('hts,shv->thv', scores, block_v)  29.3 us
    dot_general x1, matrix products, body(): jnp.dot(hidden, down_weight, preferred_element_type=jnp.float32)  13.2 us
    dynamic_update_slice x16, other arithmetic, sweep_forward(): lax.scan(advance, starting, blocks_in)  11.4 us
    another operation x4, local copies, waits for them, and re-layouts, to_blocks(): return array.reshape(block_count, blk_rows, head_count, array.shape[2])  10.1 us
    all_to_all x1, waiting for transfers between devices, body(): lax.all_to_all(readout, 'tp', split_axis=0, concat_axis=1, tiled=True)  10 us
    mul x8, other arithmetic, advance(): key_shrunk = block_k * jnp.exp(-running)  9.65 us
    mul x8, other arithmetic, advance(): query_grown = block_q * jnp.exp(suffix)  9.2 us
  transfers between devices with their start and end apart: 5, of which 2 were waited for; matrix products, arithmetic and copies ran while one was open for 45% of the time, Pallas kernels for 0%

commit v1 on v0

v1 whole, which is shorter than its diff:
```python
import functools

import jax
import jax.numpy as jnp
from jax import lax
from jax.experimental import pallas as pl
from jax.experimental.pallas import tpu as pltpu
from jax.sharding import Mesh
from jax.sharding import PartitionSpec as P

EP = ("ep_0", "ep_1")
EP_TP = ("ep_0", "ep_1", "tp")
EPSILON = 1e-06
F32, BF16 = jnp.float32, jnp.bfloat16
VMEM = pl.BlockSpec(memory_space=pltpu.VMEM)
ANY = pl.BlockSpec(memory_space=pl.ANY)
MESH = pl.DeviceIdType.MESH
BLK = 128
VMEM_MAX = 60 * 1024 * 1024


def dot(a, b):
    return jnp.dot(a, b, preferred_element_type=F32)


def dot_last(a, b):
    return lax.dot_general(a, b, (((1,), (1,)), ((), ())), preferred_element_type=F32)


def dot_first(a, b):
    return lax.dot_general(a, b, (((0,), (0,)), ((), ())), preferred_element_type=F32)


def slot_rows(routes_ref, experts, capacity):
    rows = routes_ref.shape[1]
    first, second = routes_ref[0:1, :], routes_ref[1:2, :]
    names = lax.broadcasted_iota(jnp.int32, (experts, rows), 0)
    is_first = (names == first).astype(F32)
    is_second = (names == second).astype(F32)
    earlier = lax.broadcasted_iota(jnp.int32, (rows, rows), 0) < lax.broadcasted_iota(
        jnp.int32, (rows, rows), 1
    )
    before = dot((is_first + is_second).astype(BF16), earlier.astype(F32).astype(BF16))
    base = names.astype(F32) * float(capacity) + before
    return (
        jnp.sum(is_first * base, axis=0, keepdims=True),
        jnp.sum(is_second * base, axis=0, keepdims=True),
    )


def dispatch_kernel(experts, capacity, x_ref, gain_ref, routes_ref, out_ref, own_ref):
    rows, width = x_ref.shape
    cols = out_ref.shape[1]
    mine = pl.ds(pl.multiple_of(lax.axis_index("tp") * cols, cols), cols)
    gain = gain_ref[:, mine]
    step = 32

    def norm(i, carry):
        at = pl.ds(pl.multiple_of(i * step, step), step)
        x = x_ref[at, :].astype(F32)
        factor = lax.rsqrt(jnp.sum(x * x, axis=-1, keepdims=True) * (1.0 / width) + EPSILON)
        own_ref[at, :] = (x_ref[at, mine].astype(F32) * factor * gain).astype(BF16)
        return carry

    lax.fori_loop(0, rows // step, norm, 0)
    pos_a, pos_b = slot_rows(routes_ref, experts, capacity)
    total = experts * capacity
    chunk = total // 4
    own = own_ref[...]
    for c in range(4):
        slots = (lax.broadcasted_iota(jnp.int32, (chunk, rows), 0) + c * chunk).astype(F32)
        pick = ((slots == pos_a) | (slots == pos_b)).astype(F32).astype(BF16)
        out_ref[c * chunk : (c + 1) * chunk, :] = dot(pick, own).astype(BF16)


def combine_kernel(experts, capacity, back_ref, routes_ref, logits_ref, out_ref):
    rows = routes_ref.shape[1]
    total = experts * capacity
    cols = out_ref.shape[1]
    pos_a, pos_b = slot_rows(routes_ref, experts, capacity)
    la, lb = logits_ref[0:1, :], logits_ref[1:2, :]
    wa, wb = jax.nn.sigmoid(la - lb), jax.nn.sigmoid(lb - la)
    back = back_ref[...]
    for r in range(rows // BLK):
        at = slice(r * BLK, (r + 1) * BLK)

        def column(row):
            return jnp.broadcast_to(row[:, at], (BLK, BLK)).T

        result = None
        for pos, weight in ((pos_a, wa), (pos_b, wb)):
            place = column(pos)
            lanes = lax.broadcasted_iota(jnp.int32, (BLK, BLK), 1)
            picks = [
                (place == (lanes + c * BLK).astype(F32)).astype(F32).astype(BF16)
                for c in range(total // BLK)
            ]
            got = dot(jnp.concatenate(picks, axis=1), back)
            scale = column(weight)
            term = got * jnp.concatenate([scale] * (cols // BLK), axis=1)
            result = term if result is None else result + term
        out_ref[at, :] = result.astype(BF16)


def mixer_kernel(
    x_ref,
    gain_ref,
    wq_ref,
    wf_ref,
    wb_ref,
    wv_ref,
    floor_ref,
    shift_ref,
    out_ref,
    grown_ref,
    s_ref,
    t_ref,
    n_ref,
    q_ref,
    v_ref,
    kf_ref,
    gf_ref,
    kb_ref,
    gb_ref,
    st_ref,
    off_ref,
):
    tile, width = x_ref.shape
    step_id = pl.program_id(0)
    span = 32

    def norm(i, carry):
        at = pl.ds(pl.multiple_of(i * span, span), span)
        x = x_ref[at, :].astype(F32)
        factor = lax.rsqrt(jnp.sum(x * x, axis=-1, keepdims=True) * (1.0 / width) + EPSILON)
        n_ref[at, :] = (x * factor * gain_ref[...]).astype(BF16)
        return carry

    lax.fori_loop(0, tile // span, norm, 0)
    n = n_ref[...]

    def project(w_ref):
        return dot(n, w_ref[...]).astype(BF16).astype(F32)

    at = pl.ds(pl.multiple_of(step_id * tile, tile), tile)
    u = project(wq_ref)
    q_ref[at, :] = u / (1.0 + jnp.exp(-u))
    v_ref[at, :] = project(wv_ref).astype(BF16)
    shift = []
    for j in range(tile // BLK):
        where_at = pl.ds(pl.multiple_of(step_id * tile + j * BLK, BLK), BLK)
        shift.append(
            jnp.concatenate(
                [
                    jnp.broadcast_to(shift_ref[h : h + 1, where_at], (BLK, BLK)).T
                    for h in range(2)
                ],
                axis=1,
            )
        )
    shift = jnp.concatenate(shift, axis=0)
    room = 1.0 - floor_ref[...]
    for w_ref, k_ref, g_ref in ((wf_ref, kf_ref, gf_ref), (wb_ref, kb_ref, gb_ref)):
        key = room * (1.0 - jax.nn.sigmoid(project(w_ref)))
        k_ref[at, :] = key
        g_ref[at, :] = jnp.log1p(-key) + shift

    @pl.when(step_id == pl.num_programs(0) - 1)
    def _():
        blocks = q_ref.shape[0] // BLK
        row = lax.broadcasted_iota(jnp.int32, (BLK, BLK), 0)
        col = lax.broadcasted_iota(jnp.int32, (BLK, BLK), 1)
        st_ref[...] = jnp.zeros_like(st_ref)
        off_ref[...] = jnp.zeros_like(off_ref)
        out_ref[...] = jnp.zeros_like(out_ref)

        def sweep(direction, block, k_ref, g_ref):
            rows = pl.ds(pl.multiple_of(block * BLK, BLK), BLK)
            keep = (col <= row) if direction == 0 else (col >= row)
            tri = keep.astype(F32).astype(BF16)
            g = g_ref[rows, :]
            hi = g.astype(BF16)
            lo = (g - hi.astype(F32)).astype(BF16)
            run = dot(tri, hi) + dot(tri, lo)
            end = run[BLK - 1 : BLK, :] if direction == 0 else run[0:1, :]
            mid = 0.5 * end
            half = jnp.exp(mid)
            qg = q_ref[rows, :] * jnp.exp(run - mid)
            ks = k_ref[rows, :] * jnp.exp(mid - run)
            qfull = qg * half
            kfull = (ks * half).astype(BF16)
            offset = off_ref[direction : direction + 1, :]
            grown_ref[rows, direction * 256 : direction * 256 + 256] = (
                qfull * jnp.exp(offset)
            ).astype(BF16)
            qg, ks, qfull = qg.astype(BF16), ks.astype(BF16), qfull.astype(BF16)
            decay = jnp.exp(end)
            parts = []
            for h in range(2):
                lanes = slice(h * 128, h * 128 + 128)
                v = v_ref[rows, lanes]
                state = st_ref[direction * 2 + h]
                scores = jnp.where(keep, dot_last(qg[:, lanes], ks[:, lanes]), 0.0).astype(BF16)
                parts.append(dot(scores, v) + dot_last(qfull[:, lanes], state.astype(BF16)))
                st_ref[direction * 2 + h] = state * decay[:, lanes] + dot_first(v, kfull[:, lanes])
            out_ref[rows, :] += jnp.concatenate(parts, axis=1)
            off_ref[direction : direction + 1, :] = offset + end

        def both(i, carry):
            sweep(0, i, kf_ref, gf_ref)
            sweep(1, blocks - 1 - i, kb_ref, gb_ref)
            return carry

        lax.fori_loop(0, blocks, both, 0)
        s_ref[...] = st_ref[...].astype(BF16)
        t_ref[...] = jnp.concatenate(
            [off_ref[0:1, 0:128], off_ref[0:1, 128:256], off_ref[1:2, 0:128], off_ref[1:2, 128:256]]
            + [jnp.zeros((4, 128), F32)],
            axis=0,
        )


def finish_kernel(
    s_ref,
    t_ref,
    local_ref,
    grown_ref,
    hgain_ref,
    w_hbm,
    out_ref,
    s1,
    t1,
    s2,
    t2,
    sr,
    tr,
    inc_ref,
    ro_ref,
    rin_ref,
    w_ref,
    send_a,
    recv_a,
    send_b,
    recv_b,
    send_r,
    recv_r,
    w_sem,
):
    z, x, t = lax.axis_index("ep_0"), lax.axis_index("ep_1"), lax.axis_index("tp")
    tp = rin_ref.shape[1] // 256
    w_copy = pltpu.make_async_copy(w_hbm, w_ref, w_sem)
    w_copy.start()
    barrier = pltpu.get_barrier_semaphore()
    for d in range(1, 4):
        pl.semaphore_signal(barrier, inc=1, device_id={"ep_1": lax.rem(x + d, 4)}, device_id_type=MESH)
        pl.semaphore_signal(barrier, inc=1, device_id={"ep_0": lax.rem(z + d, 4)}, device_id_type=MESH)
    for d in range(1, tp):
        pl.semaphore_signal(barrier, inc=1, device_id={"tp": lax.rem(t + d, tp)}, device_id_type=MESH)
    pl.semaphore_wait(barrier, 6 + tp - 1)

    def exchange(axis, me, s_src, t_src, s_dst, t_dst, send, recv):
        copies = []
        for d in range(1, 4):
            for n, (src, dst) in enumerate(((s_src, s_dst), (t_src, t_dst))):
                copies.append(
                    pltpu.make_async_remote_copy(
                        src_ref=src,
                        dst_ref=dst.at[d - 1],
                        send_sem=send.at[2 * d - 2 + n],
                        recv_sem=recv.at[2 * d - 2 + n],
                        device_id={axis: lax.rem(me + d, 4)},
                        device_id_type=MESH,
                    )
                )
        for c in copies:
            c.start()
        for c in copies:
            c.wait_recv()
        return copies

    def state_of(ref, n):
        return ref[n].astype(F32)

    def chain(total, log, use, s, g):
        gate = jnp.where(use, 1.0, 0.0)
        return total + gate * jnp.exp(log) * s, log + gate * g

    def walk(n, me, s_buf, t_buf, behind):
        acc, log = jnp.zeros((128, 128), F32), jnp.zeros((1, 128), F32)
        for d in (1, 2, 3) if behind else (3, 2, 1):
            use = (me >= d) if behind else (me < d)
            acc, log = chain(acc, log, use, s_buf[d - 1, n].astype(F32), t_buf[d - 1, n : n + 1, :])
        return acc, log

    first = exchange("ep_1", x, s_ref, t_ref, s1, t1, send_a, recv_a)
    near = []
    totals = []
    for n in range(4):
        forward = n < 2
        near.append(walk(n, x, s1, t1, forward))
        acc, log = jnp.zeros((128, 128), F32), jnp.zeros((1, 128), F32)
        order = (1, 2, 3) if forward else (3, 2, 1)
        for d in order:
            use = (x < d) if forward else (x >= d)
            acc, log = chain(acc, log, use, s1[d - 1, n].astype(F32), t1[d - 1, n : n + 1, :])
        acc, log = chain(acc, log, True, s_ref[n].astype(F32), t_ref[n : n + 1, :])
        for d in order:
            use = (x >= d) if forward else (x < d)
            acc, log = chain(acc, log, use, s1[d - 1, n].astype(F32), t1[d - 1, n : n + 1, :])
        sr[n] = acc.astype(BF16)
        totals.append(log)
    tr[...] = jnp.concatenate(totals + [jnp.zeros((4, 128), F32)], axis=0)
    second = exchange("ep_0", z, sr, tr, s2, t2, send_b, recv_b)
    for n in range(4):
        far, _ = walk(n, z, s2, t2, n < 2)
        acc, log = near[n]
        inc_ref[n] = (acc + jnp.exp(log) * far).astype(BF16)

    sends = []
    for d in list(range(1, tp)) + [0]:
        peer = lax.rem(t + d, tp)
        rows = pl.ds(pl.multiple_of(peer * 128, 128), 128)
        for h in range(2):
            lanes = slice(h * 128, h * 128 + 128)
            o = (
                local_ref[rows, lanes]
                + dot_last(grown_ref[rows, h * 128 : h * 128 + 128], inc_ref[h])
                + dot_last(grown_ref[rows, 256 + h * 128 : 384 + h * 128], inc_ref[2 + h])
            )
            factor = lax.rsqrt(jnp.mean(o * o, axis=-1, keepdims=True) + EPSILON)
            ro_ref[rows, lanes] = (o * factor * hgain_ref[...]).astype(BF16)
        if d:
            copy = pltpu.make_async_remote_copy(
                src_ref=ro_ref.at[rows, :],
                dst_ref=rin_ref.at[:, pl.ds(pl.multiple_of(t * 256, 256), 256)],
                send_sem=send_r.at[d - 1],
                recv_sem=recv_r.at[d - 1],
                device_id={"tp": peer},
                device_id_type=MESH,
            )
            copy.start()
            sends.append(copy)
    own = pl.ds(pl.multiple_of(t * 128, 128), 128)
    rin_ref[:, pl.ds(pl.multiple_of(t * 256, 256), 256)] = ro_ref[own, :]
    for c in sends:
        c.wait_recv()
    w_copy.wait()
    for n in range(w_ref.shape[1] // 256):
        cols = slice(n * 256, n * 256 + 256)
        out_ref[:, cols] = dot(rin_ref[...], w_ref[:, cols]).astype(BF16)
    for c in first + second + sends:
        c.wait_send()


def params(**more):
    return pltpu.CompilerParams(vmem_limit_bytes=VMEM_MAX, **more)


def body(
    mix_tokens,
    mix_gain,
    w_query,
    w_forget_fwd,
    w_forget_bwd,
    w_value,
    decay_floor,
    decay_shift,
    head_gain,
    w_out,
    moe_tokens,
    moe_gain,
    routes,
    route_logits,
    w_expert_gate,
    w_expert_up,
    w_expert_down,
):
    tp_size = lax.axis_size("tp")
    ep_size = lax.axis_size(EP)
    seg_rows, width = mix_tokens.shape
    token_rows = moe_tokens.shape[0]
    capacity = 3 * token_rows // ep_size
    part_cols = width // tp_size
    slots = ep_size * capacity
    routes_t, logits_t = routes.T, route_logits.T

    outgoing = pl.pallas_call(
        functools.partial(dispatch_kernel, ep_size, capacity),
        out_shape=jax.ShapeDtypeStruct((slots, part_cols), BF16),
        in_specs=[VMEM] * 3,
        out_specs=VMEM,
        scratch_shapes=[pltpu.VMEM((token_rows, part_cols), BF16)],
        compiler_params=params(),
        name="dispatch",
    )(moe_tokens, moe_gain.reshape(1, -1), routes_t)
    arrived = lax.all_to_all(
        outgoing.reshape(ep_size, capacity, part_cols), EP, split_axis=0, concat_axis=0, tiled=True
    )
    pieces = lax.all_gather(arrived, "tp", axis=2, tiled=True)

    tile = 256
    fixed = lambda i: (0, 0)
    local, grown, states, totals = pl.pallas_call(
        mixer_kernel,
        grid=(seg_rows // tile,),
        out_shape=(
            jax.ShapeDtypeStruct((seg_rows, 256), F32),
            jax.ShapeDtypeStruct((seg_rows, 512), BF16),
            jax.ShapeDtypeStruct((4, 128, 128), BF16),
            jax.ShapeDtypeStruct((8, 128), F32),
        ),
        in_specs=[
            pl.BlockSpec((tile, width), lambda i: (i, 0)),
            pl.BlockSpec((1, width), fixed),
            pl.BlockSpec((width, 256), fixed),
            pl.BlockSpec((width, 256), fixed),
            pl.BlockSpec((width, 256), fixed),
            pl.BlockSpec((width, 256), fixed),
            pl.BlockSpec((1, 256), fixed),
            pl.BlockSpec((2, seg_rows), fixed),
        ],
        out_specs=(
            pl.BlockSpec((seg_rows, 256), fixed),
            pl.BlockSpec((seg_rows, 512), fixed),
            pl.BlockSpec((4, 128, 128), lambda i: (0, 0, 0)),
            pl.BlockSpec((8, 128), fixed),
        ),
        scratch_shapes=[
            pltpu.VMEM((tile, width), BF16),
            pltpu.VMEM((seg_rows, 256), F32),
            pltpu.VMEM((seg_rows, 256), BF16),
            pltpu.VMEM((seg_rows, 256), F32),
            pltpu.VMEM((seg_rows, 256), F32),
            pltpu.VMEM((seg_rows, 256), F32),
            pltpu.VMEM((seg_rows, 256), F32),
            pltpu.VMEM((4, 128, 128), F32),
            pltpu.VMEM((8, 256), F32),
        ],
        compiler_params=params(dimension_semantics=("arbitrary",)),
        cost_estimate=pl.CostEstimate(flops=12 * 10**9, bytes_accessed=12 * 2**20, transcendentals=0),
        name="mixer",
    )(
        mix_tokens,
        mix_gain.reshape(1, -1),
        w_query,
        w_forget_fwd,
        w_forget_bwd,
        w_value,
        decay_floor.reshape(1, -1),
        decay_shift.T,
    )
    mixed_out = pl.pallas_call(
        finish_kernel,
        out_shape=jax.ShapeDtypeStruct((seg_rows // tp_size, width), BF16),
        in_specs=[VMEM, VMEM, VMEM, VMEM, VMEM, ANY],
        out_specs=VMEM,
        scratch_shapes=[
            pltpu.VMEM((3, 4, 128, 128), BF16),
            pltpu.VMEM((3, 8, 128), F32),
            pltpu.VMEM((3, 4, 128, 128), BF16),
            pltpu.VMEM((3, 8, 128), F32),
            pltpu.VMEM((4, 128, 128), BF16),
            pltpu.VMEM((8, 128), F32),
            pltpu.VMEM((4, 128, 128), BF16),
            pltpu.VMEM((seg_rows, 256), BF16),
            pltpu.VMEM((seg_rows // tp_size, width), BF16),
            pltpu.VMEM(w_out.shape, BF16),
            pltpu.SemaphoreType.DMA((6,)),
            pltpu.SemaphoreType.DMA((6,)),
            pltpu.SemaphoreType.DMA((6,)),
            pltpu.SemaphoreType.DMA((6,)),
            pltpu.SemaphoreType.DMA((tp_size - 1,)),
            pltpu.SemaphoreType.DMA((tp_size - 1,)),
            pltpu.SemaphoreType.DMA,
        ],
        compiler_params=params(collective_id=1, has_side_effects=True),
        cost_estimate=pl.CostEstimate(flops=12 * 10**9, bytes_accessed=12 * 2**20, transcendentals=0),
        name="finish",
    )(states, totals, local, grown, head_gain.reshape(1, -1), w_out)

    flattened = pieces.reshape(-1, width)
    gate_acts = dot(flattened, w_expert_gate[0])
    up_acts = dot(flattened, w_expert_up[0])
    hidden = (jax.nn.silu(gate_acts) * up_acts).astype(BF16)
    partial_value = dot(hidden, w_expert_down[0])
    summed = lax.psum_scatter(partial_value.astype(BF16), "tp", scatter_dimension=1, tiled=True)
    returned = lax.all_to_all(
        summed.reshape(ep_size, capacity, part_cols), EP, split_axis=0, concat_axis=0, tiled=True
    )
    moe_out = pl.pallas_call(
        functools.partial(combine_kernel, ep_size, capacity),
        out_shape=jax.ShapeDtypeStruct((token_rows, part_cols), BF16),
        in_specs=[VMEM] * 3,
        out_specs=VMEM,
        compiler_params=params(),
        name="combine",
    )(returned.reshape(slots, part_cols), routes_t, logits_t)
    return (mixed_out, moe_out)


def solution(mesh):
    finer = Mesh(mesh.devices.reshape(4, 4, mesh.shape["tp"]), ("ep_0", "ep_1", "tp"))
    return jax.shard_map(
        body,
        mesh=finer,
        in_specs=(
            P(EP, None),
            P(),
            P(None, "tp"),
            P(None, "tp"),
            P(None, "tp"),
            P(None, "tp"),
            P("tp"),
            P(EP, "tp"),
            P(),
            P(),
            P(EP, None),
            P(),
            P(EP, None),
            P(EP, None),
            P(EP, None, "tp"),
            P(EP, None, "tp"),
            P(EP, "tp", None),
        ),
        out_specs=(P(EP_TP, None), P(EP, "tp")),
        check_vma=False,
    )
```

time: 333 us -> 185 us (0.56)
  other arithmetic: 70.3 us -> 0 us
  matrix products: 86.5 us -> 21.7 us
  blocking collectives: 83.3 us -> 20.4 us
  Pallas kernels: 0 us -> 61.9 us
  waiting for transfers between devices: 15.4 us -> 54.8 us
  local copies, waits for them, and re-layouts: 41.6 us -> 2.7 us
  starting transfers between devices: 17.8 us -> 7.04 us
    all_gather x8 -> x0, blocking collectives: 83.3 us -> none  [prefix_by_axis(): lax.all_gather(part.astype(kind), axis)]
    dot_general x56 -> x2, matrix products: 86.5 us -> 21.7 us  [dot(): return jnp.dot(a, b, preferred_element_type=F32)]
    pallas_call x0 -> x4, Pallas kernels: none -> 61.9 us  [the longest x1 33.7 us: body(): pl.pallas_call(finish_kernel, out_shape=jax.ShapeDtypeStruct((seg_rows //...]
    all_gather x1, waiting for transfers between devices: 0.02 us -> 35.7 us  [body(): pieces = lax.all_gather(arrived, 'tp', axis=2, tiled=True)]
    all_to_all x0 -> x1, blocking collectives: none -> 20.4 us  [body(): lax.all_to_all(outgoing.reshape(ep_size, capacity, part_cols), EP, split_...]
    reduce_scatter x1, waiting for transfers between devices: 0.01 us -> 19.1 us  [body(): lax.psum_scatter(partial_value.astype(BF16), 'tp', scatter_dimension=1, t...]
    mul x17 -> x0, other arithmetic: 19 us -> none  [the longest x8 9.65 us: advance(): key_shrunk = block_k * jnp.exp(-running)]
    another operation x18 -> x0, other arithmetic: 18.7 us -> none  [the longest x8 8.64 us: advance(): suffix = block_sum[None] - jnp.cumsum(block_g, axis=0) + block_g]
  transfers between devices with their start and end apart: 5 -> 3, of which waited for: 2 -> 2; matrix products, arithmetic and copies ran while one was open for 45% -> 0% of each run, Pallas kernels for 0% -> 30%
where the time goes in v1:
time: 185 us; the launch traced here: 183 us
  Pallas kernels  61.9 us (33%)
  waiting for transfers between devices  54.8 us (30%)
  matrix products  21.7 us (12%)
  blocking collectives  20.4 us (11%)
  between operations  14.1 us (8%)
  starting transfers between devices  7.04 us (4%)
  local copies, waits for them, and re-layouts  2.7 us (1%)
    all_gather x1, waiting for transfers between devices, body(): pieces = lax.all_gather(arrived, 'tp', axis=2, tiled=True)  35.7 us
    pallas_call x1, Pallas kernels, body(): pl.pallas_call(finish_kernel, out_shape=jax.ShapeDtypeStruct((seg_rows //...  33.7 us
    dot_general x2, matrix products, dot(): return jnp.dot(a, b, preferred_element_type=F32)  21.7 us
    pallas_call x1, Pallas kernels, body(): pl.pallas_call(mixer_kernel, grid=(seg_rows // tile,), out_shape=(jax.Sha...  21.1 us
    all_to_all x1, blocking collectives, body(): lax.all_to_all(outgoing.reshape(ep_size, capacity, part_cols), EP, split_...  20.4 us
    reduce_scatter x1, waiting for transfers between devices, body(): lax.psum_scatter(partial_value.astype(BF16), 'tp', scatter_dimension=1, t...  19.1 us
    all_to_all x1, starting transfers between devices, body(): lax.all_to_all(summed.reshape(ep_size, capacity, part_cols), EP, split_ax...  6.96 us
    pallas_call x1, Pallas kernels, body(): pl.pallas_call(functools.partial(dispatch_kernel, ep_size, capacity), out...  4.47 us
  transfers between devices with their start and end apart: 3, of which 2 were waited for; matrix products, arithmetic and copies ran while one was open for 0% of the time, Pallas kernels for 30%

profile of v1, /device:TPU:0, one launch (start us, length us, event | category | flops | bytes accessed | tf_op | source)
XLA Modules:
  0.0 182.7 jit_solution(16431033952349362574)
XLA Ops:
  7.2 0.0 copy-start
  7.2 0.0 all-gather.2.cloned.1.call-start
  7.2 4.5 %dispatch.1 = bf16[1152,256]{1,0:T(8,128)(2,1)} custom-call(bf16[384,2048]{1,0:T(8,128)(2,1)} %x_ref.3, f32[1,2048]{1,0:T(1,128)} %bitcast.29, s32[2,384]{1,0:T(2,128)} %bitcast.27), custom_call_target="tpu_custom_call" | custom-call | tf_op jit(solution)/shard_map/dispatch/pallas_call | solution.py:387
  11.7 20.4 %all_to_all.10 = bf16[16,72,256]{2,1,0:T(8,128)(2,1)} all-to-all(bf16[16,72,256]{2,1,0:T(8,128)(2,1)} %bitcast.24), channel_id=1, replica_groups=mesh['ep_0'=4,'ep_1'=4,'tp'=8] {'ep_0','ep_1'}, dimensions={0} | all-to-all | bytes 1179648 | tf_op jit(solution)/shard_map/all_to_all | solution.py:396
  32.1 0.0 all-gather.2.cloned.1.call-update
  32.1 0.0 reduce-scatter.2.cloned.1.call-start
  32.1 35.7 %all-gather.2.cloned.1.call-done = bf16[16,72,2048]{2,1,0:T(8,128)(2,1)} async-done(((bf16[16,72,256]{2,1,0:T(8,128)(2,1)}), bf16[16,72,2048]{2,1,0:T(8,128)(2,1)}) %all-gather.2.cloned.1.call-update) | async-done | bytes 4718608 | tf_op jit(solution)/shard_map/all_gather | solution.py:399
  67.8 8.6 %fusion.3 = f32[1152,640]{1,0:T(8,128)} fusion(bf16[1152,2048]{1,0:T(8,128)(2,1)} %bitcast.31, bf16[1,2048,640]{2,1,0:T(8,128)(2,1)} %param.31), kind=kOutput, calls=%fused_computation.5 | convolution fusion | flops 3019898880 | bytes 10289152 | tf_op jit(solution)/shard_map/dot_general | solution.py:23
  76.4 0.0 copy-done
  76.4 13.2 %convolution_convert_fusion = bf16[1152,2048]{1,0:T(8,128)(2,1)} fusion(bf16[1,640,2048]{2,1,0:T(8,128)(2,1)S(1)} %copy-done, bf16[1152,2048]{1,0:T(8,128)(2,1)} %bitcast.32, f32[1152,640]{1,0:T(8,128)} %fusion.3, bf16[1,2048,640]{2,1,0:T(8,128)(2,1)} %param.32), kind=kOutput, calls=%fused_computation | convolution fusion | flops 6046580736 | bytes 17629184 | tf_op jit(solution)/shard_map/dot_general | solution.py:23
  89.6 0.0 reduce-scatter.2.cloned.1.call-update
  89.6 21.1 %mixer.1 = (f32[1024,256]{1,0:T(8,128)}, bf16[1024,512]{1,0:T(8,128)(2,1)}, bf16[4,128,128]{2,1,0:T(8,128)(2,1)}, f32[8,128]{1,0:T(8,128)}) custom-call(bf16[1024,2048]{1,0:T(8,128)(2,1)} %x_ref.2, f32[1,2048]{1,0:T(1,128)} %bitcast.33, bf16[2048,256]{1,0:T(8,128)(2,1)} %wq_ref.1, bf16[2048,256]{1,0:T(8,128)(2,1)} %wf_ref.1, bf16[2048,256]{1,0:T(8,128)(2,1)} %wb_ref.1, ...), custom_call_target="tpu_custom_call" | custom-call | flops 12000000000 | bytes 12582912 | tf_op jit(solution)/shard_map/mixer/pallas_call | solution.py:403
  110.7 19.1 %reduce-scatter.2.cloned.1.call-done = bf16[1152,256]{1,0:T(8,128)(2,1)} async-done(((bf16[1152,2048]{1,0:T(8,128)(2,1)}), bf16[1152,256]{1,0:T(8,128)(2,1)}) %reduce-scatter.2.cloned.1.call-update) | async-done | bytes 589840 | tf_op jit(solution)/shard_map/reduce_scatter | solution.py:486
  129.8 7.0 %all-to-all-start.1 = ((bf16[16,72,256]{2,1,0:T(8,128)(2,1)}), bf16[16,72,256]{2,1,0:T(8,128)(2,1)S(1)}, u32[]{:S(2)}, u32[]{:S(2)}) async-start(bf16[16,72,256]{2,1,0:T(8,128)(2,1)} %bitcast.26), calls=%async_computation.2 | async-start | bytes 1179648 | tf_op jit(solution)/shard_map/all_to_all | solution.py:487
  136.8 33.7 %finish.1 = bf16[128,2048]{1,0:T(8,128)(2,1)} custom-call(bf16[4,128,128]{2,1,0:T(8,128)(2,1)} %get-tuple-element.6.s_ref, f32[8,128]{1,0:T(8,128)} %get-tuple-element.7.t_ref, f32[1024,256]{1,0:T(8,128)} %get-tuple-element.8.local_ref, bf16[1024,512]{1,0:T(8,128)(2,1)} %get-tuple-element.9.grown_ref, f32[1,128]{1,0:T(1,128)} %bitcast.36, ...), custom_call_target="tpu_custom_call" | custom-call | flops 12000000000 | bytes 12582912 | tf_op jit(solution)/shard_map/finish/pallas_call | solution.py:452
  170.5 0.0 all-to-all-done.1
  170.5 0.0 copy-start.1
  170.5 0.8 copy-done.1
  171.3 2.6 %combine.1 = bf16[384,256]{1,0:T(8,128)(2,1)} custom-call(bf16[1152,256]{1,0:T(8,128)(2,1)} %bitcast.25, s32[2,384]{1,0:T(2,128)} %bitcast.28, f32[2,384]{1,0:T(2,128)} %bitcast.30), custom_call_target="tpu_custom_call" | custom-call | tf_op jit(solution)/shard_map/combine/pallas_call | solution.py:490
  173.9 1.9 %copy.20 = bf16[128,2048]{1,0:T(8,128)(2,1)} copy(bf16[128,2048]{1,0:T(8,128)(2,1)} %finish.1) | data formatting | bytes 1048576
Async XLA Ops:
  7.2 69.2 %copy-start = (bf16[1,640,2048]{2,1,0:T(8,128)(2,1)S(1)}, bf16[1,640,2048]{2,1,0:T(8,128)(2,1)}, u32[]{:S(2)}) copy-start(bf16[1,640,2048]{2,1,0:T(8,128)(2,1)} %param.33) | copy-start | bytes 7864324
  7.2 60.6 %all-gather.2.cloned.1.call-start = ((), (), s32[]{:S(2)}) async-start(), calls=%async_computation.3 | async-start | bytes 5308416 | tf_op jit(solution)/shard_map/all_gather | solution.py:399
  32.1 97.7 %reduce-scatter.2.cloned.1.call-start = ((), (), s32[]{:S(2)}) async-start(), calls=%async_computation.4 | async-start | bytes 5308416 | tf_op jit(solution)/shard_map/reduce_scatter | solution.py:486
  129.8 40.6 %all-to-all-start.1 = ((bf16[16,72,256]{2,1,0:T(8,128)(2,1)}), bf16[16,72,256]{2,1,0:T(8,128)(2,1)S(1)}, u32[]{:S(2)}, u32[]{:S(2)}) async-start(bf16[16,72,256]{2,1,0:T(8,128)(2,1)} %bitcast.26), calls=%async_computation.2 | async-start | bytes 1179648 | tf_op jit(solution)/shard_map/all_to_all | solution.py:487
  170.5 0.8 copy-start.1
Sparse Core Ops, SparseCore 0:
  32.2 35.5 all-gather.1
  89.7 40.0 reduce-scatter.1
